TPU v7x, 512 devices: a whole 4x4x16 slice. The times are simulated.
512 devices in a mesh: sp: 32 (over z, core), tp: 16 (over y, x).
Axes of the slice: x: 4, y: 4, z: 16, core: 2. Of those that a mesh axis runs over, the one named last changes fastest.
Arguments:
- queries: bfloat16 [8192, 2048], P('sp', 'tp'), may hold values from -6 to 6
- keys: bfloat16 [8192, 256], P('sp'), may hold values from -6 to 6
- values: bfloat16 [8192, 256], P('sp'), may hold values from -6 to 6
- query_gain: float32 [128], replicated, may hold values from 0.1 to 5.5
- key_gain: float32 [128], replicated, may hold values from 0.1 to 5.5
- out_proj: bfloat16 [2048, 2048], P(None, 'tp'), may hold values from -0.125 to 0.125
- expert_norm_scale: float32 [2048], replicated, may hold values from 0.1 to 1.9
- residual: bfloat16 [8192, 2048], P(('sp', 'tp')), may hold values from -6 to 6
- routes: int32 [8192, 2], P(('sp', 'tp')), may hold values from 0 to 31, all different within a row; in each aligned block of 16 rows (0 to 15, 16 to 31, ...) at most 2 rows name the same one
- route_weights: float32 [8192, 2], P(('sp', 'tp')), may hold values from 0.1 to 0.9
- w_gate: bfloat16 [32, 2048, 4096], P('sp', None, 'tp'), may hold values from -0.125 to 0.125
- w_up: bfloat16 [32, 2048, 4096], P('sp', None, 'tp'), may hold values from -0.125 to 0.125
- w_down: bfloat16 [32, 4096, 2048], P('sp', 'tp'), may hold values from -0.09375 to 0.09375
Outputs:
- layer_out: bfloat16 [8192, 2048], P(('sp', 'tp'))
Inputs may be any that keep to these rules, and one draw needn't show every extreme that they name: `routes`: in the rows of one device no expert is named by more than 2 rows, a bound that some block reaches; a row names 2 different experts.
All inputs are finite; a program needn't handle non-finite values.
Results may differ from a plain program's by a relative error of at most 0.0095.
The roundings to bfloat16 on the way count: a program that leaves them out, or rounds other values in their place, can miss the bound.
Values may be sent and summed in bfloat16 or wider, within the bound.
No kernel may reach another device: no remote copies, remote signals or barrier semaphores. Data moves between devices by JAX's collectives and lax.ppermute only.
A program may use at most 64 MiB of HBM per device.

v0:
```python
import jax
import jax.numpy as jnp
from jax import lax
from jax.sharding import PartitionSpec as P

GRID_W = 64
EPS = 1e-06
ROPE_BASE = 10000.0
NEG_START = -1e30


def side_by_side(arrays, axis, dim, along):
    both = jnp.concatenate(arrays, axis=along)
    result, at, done = (lax.all_gather(both, axis, axis=dim, tiled=True), 0, [])
    for a in arrays:
        done.append(lax.slice_in_dim(result, at, at + a.shape[along], axis=along))
        at += a.shape[along]
    return tuple(done)


def joined_along(tiles, dim):
    dims = list(tiles.shape[1:])
    dims[dim] *= tiles.shape[0]
    return jnp.moveaxis(tiles, 0, dim).reshape(dims)


def copy_for_each(value, axis):
    copies = jnp.broadcast_to(value, (lax.axis_size(axis), *value.shape))
    return lax.all_to_all(copies, axis, split_axis=0, concat_axis=0, tiled=True)


def gather_directly(value, axis, dim):
    return joined_along(copy_for_each(value, axis), dim)


def split_up(value, dim, peers):
    before, after = (value.shape[:dim], value.shape[dim + 1 :])
    return jnp.moveaxis(value.reshape(*before, peers, -1, *after), dim, 0)


def sent_and_summed(value, axis, dim):
    peers = lax.axis_size(axis)
    tiles = lax.all_to_all(split_up(value, dim, peers), axis, 0, 0, tiled=True)
    return jnp.sum(tiles.astype(jnp.float32), axis=0)


def rotate(field, position):
    half = field.shape[-1] // 2
    quarter = half // 2
    freqs = ROPE_BASE ** (-jnp.arange(quarter, dtype=jnp.float32) / quarter)
    grid_row = (position // GRID_W).astype(jnp.float32)
    grid_col = (position % GRID_W).astype(jnp.float32)

    def turn_half(part, coord):
        angle = coord[:, None] * freqs[None, :]
        cosine = jnp.cos(angle)[:, None, :]
        sine = jnp.sin(angle)[:, None, :]
        first, second = (part[..., :quarter], part[..., quarter:])
        return jnp.concatenate(
            [first * cosine - second * sine, second * cosine + first * sine], axis=-1
        )

    return jnp.concatenate(
        [turn_half(field[..., :half], grid_row), turn_half(field[..., half:], grid_col)], axis=-1
    )


def prepare(field, gain, position):
    count = field.shape[0]
    width = gain.shape[0]
    heads_here = field.shape[1] // width
    values_f = field.reshape(count, heads_here, width).astype(jnp.float32)
    scaled = (
        values_f * lax.rsqrt(jnp.mean(values_f * values_f, axis=-1, keepdims=True) + EPS) * gain
    )
    return rotate(scaled, position).reshape(count, heads_here * width).astype(jnp.bfloat16)


def absorb(carry, query_matrix, key_rows, value_rows, scale):
    count = key_rows.shape[0]
    width = 2048
    key_blocks = key_rows.reshape(count // width, width, key_rows.shape[1], key_rows.shape[2])
    value_blocks = value_rows.reshape(
        count // width, width, value_rows.shape[1], value_rows.shape[2]
    )

    def step(state, block):
        run_max, run_sum, run_acc = state
        key_tile_rows, value_tile_rows = block
        scores = (
            jnp.einsum(
                "hxt,ght->hxg", query_matrix, key_tile_rows, preferred_element_type=jnp.float32
            )
            * scale
        )
        new_max = jnp.maximum(run_max, jnp.max(scores, axis=-1))
        weight_tensors = jnp.exp(scores - new_max[..., None]).astype(jnp.bfloat16)
        factor = jnp.exp(run_max - new_max)
        run_sum = run_sum * factor + jnp.sum(weight_tensors.astype(jnp.float32), axis=-1)
        run_acc = run_acc * factor[..., None] + jnp.einsum(
            "zij,jzu->ziu", weight_tensors, value_tile_rows, preferred_element_type=jnp.float32
        )
        return ((new_max, run_sum, run_acc), None)

    result, unused = lax.scan(step, carry, (key_blocks, value_blocks))
    return result


def start_state(batch, rows, width):
    return (
        jnp.full((batch, rows), NEG_START, jnp.float32),
        jnp.zeros((batch, rows), jnp.float32),
        jnp.zeros((batch, rows, width), jnp.float32),
    )


def local(
    queries,
    keys,
    values,
    query_gain,
    key_gain,
    out_proj,
    expert_norm_scale,
    residual,
    routes,
    route_weights,
    w_gate,
    w_up,
    w_down,
):
    head_size = query_gain.shape[0]
    tok_sp = queries.shape[0]
    tp_count = lax.axis_size("tp")
    sp_count = lax.axis_size("sp")
    heads_dev = queries.shape[1] // head_size
    all_heads = heads_dev * tp_count
    kv_heads = keys.shape[1] // head_size
    group = all_heads // kv_heads
    scale = head_size ** (-0.5)
    tp_index = lax.axis_index("tp")
    sp_index = lax.axis_index("sp")
    position = sp_index * tok_sp + jnp.arange(tok_sp, dtype=jnp.int32)
    q_rot = prepare(queries, query_gain, position)
    shared_value_head = tp_index * heads_dev // group
    own_keys = prepare(
        lax.dynamic_slice_in_dim(keys, shared_value_head * head_size, head_size, 1),
        key_gain,
        position,
    )
    own_values = lax.dynamic_slice_in_dim(values, shared_value_head * head_size, head_size, 1)
    query_matrix = q_rot.reshape(tok_sp, heads_dev, head_size).transpose(1, 0, 2)
    key_piece, value_piece = side_by_side((own_keys, own_values), "sp", 0, 1)
    run_max, run_sum, run_acc = absorb(
        start_state(1, heads_dev * tok_sp, head_size),
        query_matrix,
        key_piece[:, None, :],
        value_piece[:, None, :],
        scale,
    )
    attn = (run_acc / run_sum[..., None]).astype(jnp.bfloat16)
    attn = attn.transpose(1, 0, 2).reshape(tok_sp, heads_dev * head_size)
    columns = jnp.dot(gather_directly(attn, "tp", 1), out_proj, preferred_element_type=jnp.float32)
    projected = lax.all_to_all(
        columns.astype(jnp.bfloat16), "tp", split_axis=0, concat_axis=1, tiled=True
    )
    mixed_float_output = residual.astype(jnp.float32) + projected.astype(jnp.float32)
    mixed = mixed_float_output.astype(jnp.bfloat16)
    mixed_float_output = mixed.astype(jnp.float32)
    normed = (
        mixed_float_output
        * lax.rsqrt(jnp.mean(mixed_float_output * mixed_float_output, axis=-1, keepdims=True) + EPS)
        * expert_norm_scale
    ).astype(jnp.bfloat16)
    tok_dev = residual.shape[0]
    top = routes.shape[1]
    capacity = max(2, 2 * tok_dev * top // sp_count)
    flat_routes = routes.reshape(-1)
    one_hot = (flat_routes[:, None] == jnp.arange(sp_count, dtype=jnp.int32)[None, :]).astype(
        jnp.int32
    )
    earlier = jnp.cumsum(one_hot, axis=0) - one_hot
    slot_index = jnp.sum(earlier * one_hot, axis=1)
    target = flat_routes * capacity + slot_index
    selector = (
        jnp.arange(sp_count * capacity, dtype=jnp.int32)[:, None] == target[None, :]
    ).astype(jnp.bfloat16)
    selector = jnp.sum(selector.reshape(sp_count * capacity, tok_dev, top), axis=2)
    send_rows = jnp.dot(selector, normed, preferred_element_type=jnp.float32).astype(jnp.bfloat16)
    arrived = lax.all_to_all(send_rows, "sp", split_axis=0, concat_axis=0, tiled=True)
    gate_weight = w_gate[0]
    up_weight = w_up[0]
    down_weight = w_down[0]
    piece = lax.all_gather(arrived, "tp", axis=0, tiled=True)
    gate = jnp.dot(piece, gate_weight, preferred_element_type=jnp.float32)
    upper = jnp.dot(piece, up_weight, preferred_element_type=jnp.float32)
    hidden = (jax.nn.silu(gate) * upper).astype(jnp.bfloat16)
    expert_out = sent_and_summed(
        jnp.dot(hidden, down_weight, preferred_element_type=jnp.float32).astype(jnp.bfloat16),
        "tp",
        0,
    ).astype(jnp.bfloat16)
    returned = lax.all_to_all(expert_out, "sp", split_axis=0, concat_axis=0, tiled=True)
    picked = (
        jnp.take(returned, target, axis=0)
        .astype(jnp.float32)
        .reshape(tok_dev, top, returned.shape[1])
    )
    moe_sum = jnp.sum(picked * route_weights[:, :, None], axis=1)
    return (mixed_float_output + moe_sum).astype(jnp.bfloat16)


def solution(mesh):
    placed = (
        P("sp", "tp"),
        P("sp", None),
        P("sp", None),
        P(),
        P(),
        P(None, "tp"),
        P(),
        P(("sp", "tp"), None),
        P(("sp", "tp"), None),
        P(("sp", "tp"), None),
        P("sp", None, "tp"),
        P("sp", None, "tp"),
        P("sp", "tp", None),
    )
    return jax.shard_map(
        local, mesh=mesh, in_specs=placed, out_specs=P(("sp", "tp"), None), check_vma=False
    )
```

profile of v0, /device:TPU:1, one launch (start us, length us, event | category | flops | bytes accessed | tf_op | source)
XLA Modules:
  0.0 363.4 jit_solution(8110786324239800701)
XLA Ops:
  11.5 86.4 %all-gather.3.cloned.1.call-done = bf16[8192,256]{0,1:T(8,128)(2,1)} async-done(((bf16[256,256]{0,1:T(8,128)(2,1)}), bf16[8192,256]{0,1:T(8,128)(2,1)}) %all-gather.3.cloned.1.call-update) | async-done | bytes 4194320 | tf_op jit(solution)/shard_map/all_gather | solution.py:14
  97.9 3.9 %fusion.82 = (bf16[8192,128]{0,1:T(8,128)(2,1)S(1)}, bf16[8192,128]{0,1:T(8,128)(2,1)}) fusion(bf16[8192,256]{0,1:T(8,128)(2,1)} %all-gather.3.cloned.1.call-done), kind=kLoop, calls=%fused_computation.132 | loop fusion | bytes 8388608 | tf_op jit(solution)/shard_map/slice | solution.py:16
  101.8 4.1 %copy.35 = bf16[8192,128]{1,0:T(8,128)(2,1)} copy(bf16[8192,128]{0,1:T(8,128)(2,1)} %get-tuple-element.113) | data formatting | bytes 4194304 | tf_op jit(solution)/shard_map/slice | solution.py:16
  105.9 2.4 copy.37
  108.4 14.2 %while.15 = (s32[]{:T(128)}, f32[1,256]{1,0:T(1,128)S(1)}, f32[1,256]{1,0:T(1,128)S(1)}, f32[1,256,128]{2,1,0:T(8,128)S(1)}, bf16[4,2048,1,128]{3,1,2,0:T(8,128)...) while((s32[]{:T(128)}, f32[1,256]{1,0:T(1,128)S(1)}, ...), condition=%wide.region_5.6_spmd.clone, body=%wide.region_2.5_spmd.clone.sunk | while | flops 272729344 | bytes 7685225 | solution.py:105
  110.3 1.6 fusion.97
  111.9 1.6 fusion.94
  113.9 1.6 fusion.97
  115.5 1.6 fusion.94
  117.4 1.6 fusion.97
  119.0 1.6 fusion.94
  121.0 1.6 fusion.97
  123.9 6.7 %all-to-all-start = ((bf16[16,256,128]{1,2,0:T(8,128)(2,1)}), bf16[16,256,128]{1,2,0:T(8,128)(2,1)S(1)}, u32[]{:S(2)}, u32[]{:S(2)}) async-start(bf16[16,256,128]{1,2,0:T(8,128)(2,1)} %broadcast_in_dim.18), calls=%async_computation | async-start | bytes 2097152 | tf_op jit(solution)/shard_map/all_to_all | solution.py:29
  131.3 15.7 %all-to-all-done = bf16[16,256,128]{1,2,0:T(8,128)(2,1)S(1)} async-done(((bf16[16,256,128]{1,2,0:T(8,128)(2,1)}), bf16[16,256,128]{1,2,0:T(8,128)(2,1)S(1)}, u32[]{:S(2)}, u32[]{:S(2)}) %all-to-all-start) | async-done | bytes 1048608 | tf_op jit(solution)/shard_map/all_to_all | solution.py:29
  148.1 4.5 %all-to-all-start.1 = ((bf16[16,16,128]{2,1,0:T(8,128)(2,1)}), bf16[16,16,128]{2,1,0:T(8,128)(2,1)S(1)}, u32[]{:S(2)}, u32[]{:S(2)}) async-start(bf16[16,16,128]{2,1,0:T(8,128)(2,1)} %bitcast.12), calls=%async_computation.1 | async-start | bytes 131072 | tf_op jit(solution)/shard_map/all_to_all | solution.py:164
  152.8 6.4 %all-to-all-done.1 = bf16[16,16,128]{2,1,0:T(8,128)(2,1)S(1)} async-done(((bf16[16,16,128]{2,1,0:T(8,128)(2,1)}), bf16[16,16,128]{2,1,0:T(8,128)(2,1)S(1)}, u32[]{:S(2)}, u32[]{:S(2)}) %all-to-all-start.1) | async-done | bytes 65568 | tf_op jit(solution)/shard_map/all_to_all | solution.py:164
  159.8 30.5 %all_to_all.47 = bf16[32,2,2048]{2,1,0:T(2,128)(2,1)S(1)} all-to-all(bf16[32,2,2048]{2,1,0:T(2,128)(2,1)S(1)} %all_to_all.35), channel_id=1, replica_groups=mesh['sp'=32,'tp'=16] {'sp'}, dimensions={0} | all-to-all | bytes 524288 | tf_op jit(solution)/shard_map/all_to_all | solution.py:190
  191.1 54.4 %all-gather.5.cloned.1.call-done = bf16[1024,2048]{1,0:T(8,128)(2,1)} async-done(((bf16[64,2048]{1,0:T(8,128)(2,1)}), bf16[1024,2048]{1,0:T(8,128)(2,1)}) %all-gather.5.cloned.1.call-update) | async-done | bytes 4194320 | tf_op jit(solution)/shard_map/all_gather | solution.py:194
  245.5 4.5 %fusion.15 = f32[1024,256]{1,0:T(8,128)} fusion(bf16[1024,2048]{1,0:T(8,128)(2,1)} %all-gather.5.cloned.1.call-done, bf16[1,2048,256]{2,1,0:T(8,128)(2,1)S(1)} %copy-done.6), kind=kOutput, calls=%fused_computation.27 | convolution fusion | flops 1073741824 | bytes 6291456 | tf_op jit(solution)/shard_map/dot_general | solution.py:195
  250.0 9.1 %convolution_convert_fusion = bf16[1024,2048]{1,0:T(8,128)(2,1)} fusion(bf16[1024,2048]{1,0:T(8,128)(2,1)} %all-gather.5.cloned.1.call-done, bf16[1,256,2048]{2,1,0:T(8,128)(2,1)S(1)} %copy-done, bf16[1,2048,256]{2,1,0:T(8,128)(2,1)} %param.26, f32[1024,256]{1,0:T(8,128)} %fusion.15), kind=kOutput, calls=%fused_computation.20 | convolution fusion | flops 2151153664 | bytes 11534336 | tf_op jit(solution)/shard_map/dot_general | solution.py:199
  259.1 55.0 %all_to_all.48 = bf16[16,64,2048]{2,1,0:T(8,128)(2,1)} all-to-all(bf16[16,64,2048]{2,1,0:T(8,128)(2,1)} %bitcast.91), channel_id=1, replica_groups=mesh['sp'=32,'tp'=16] {'tp'}, dimensions={0} | all-to-all | bytes 8388608 | tf_op jit(solution)/shard_map/all_to_all | solution.py:43
  314.1 3.0 reduce_sum.90
  317.9 14.3 %all-to-all-start.4 = ((bf16[32,2,2048]{2,1,0:T(2,128)(2,1)}), bf16[32,2,2048]{2,1,0:T(2,128)(2,1)S(1)}, u32[]{:S(2)}, u32[]{:S(2)}) async-start(bf16[32,2,2048]{2,1,0:T(2,128)(2,1)} %all_to_all.39), calls=%async_computation.4 | async-start | bytes 524288 | tf_op jit(solution)/shard_map/all_to_all | solution.py:203
  332.6 21.9 %all-to-all-done.4 = bf16[32,2,2048]{2,1,0:T(2,128)(2,1)S(1)} async-done(((bf16[32,2,2048]{2,1,0:T(2,128)(2,1)}), bf16[32,2,2048]{2,1,0:T(2,128)(2,1)S(1)}, u32[]{:S(2)}, u32[]{:S(2)}) %all-to-all-start.4) | async-done | bytes 262176 | tf_op jit(solution)/shard_map/all_to_all | solution.py:203
  (86 shorter events, 15.9 us)
Async XLA Ops:
  6.5 243.5 %copy-start = (bf16[1,256,2048]{2,1,0:T(8,128)(2,1)S(1)}, bf16[1,256,2048]{2,1,0:T(8,128)(2,1)}, u32[]{:S(2)}) copy-start(bf16[1,256,2048]{2,1,0:T(8,128)(2,1)} %param.27) | copy-start | bytes 3145732
  6.5 91.4 %all-gather.3.cloned.1.call-start = ((), (), s32[]{:S(2)}) async-start(), calls=%async_computation.5 | async-start | bytes 4325376 | tf_op jit(solution)/shard_map/all_gather | solution.py:14
  122.6 8.0 %copy-start.3 = (s32[16,2]{0,1:T(2,128)S(1)}, s32[16,2]{0,1:T(2,128)}, u32[]{:S(2)}) copy-start(s32[16,2]{0,1:T(2,128)} %param.23) | copy-start | bytes 388
  122.6 24.4 %copy-start.1 = (bf16[2048,128]{1,0:T(8,128)(2,1)S(1)}, bf16[2048,128]{1,0:T(8,128)(2,1)}, u32[]{:S(2)}) copy-start(bf16[2048,128]{1,0:T(8,128)(2,1)} %param.20) | copy-start | bytes 1572868
  123.9 35.2 %copy-start.2 = (bf16[16,2048]{1,0:T(8,128)(2,1)S(1)}, bf16[16,2048]{1,0:T(8,128)(2,1)}, u32[]{:S(2)}) copy-start(bf16[16,2048]{1,0:T(8,128)(2,1)} %param.22) | copy-start | bytes 196612
  123.9 35.4 %copy-start.4 = (f32[2048]{0:T(1024)S(1)}, f32[2048]{0:T(1024)}, u32[]{:S(2)}) copy-start(f32[2048]{0:T(1024)} %param.21) | copy-start | bytes 24580
  123.9 23.1 %all-to-all-start = ((bf16[16,256,128]{1,2,0:T(8,128)(2,1)}), bf16[16,256,128]{1,2,0:T(8,128)(2,1)S(1)}, u32[]{:S(2)}, u32[]{:S(2)}) async-start(bf16[16,256,128]{1,2,0:T(8,128)(2,1)} %broadcast_in_dim.18), calls=%async_computation | async-start | bytes 2097152 | tf_op jit(solution)/shard_map/all_to_all | solution.py:29
  148.1 11.0 %all-to-all-start.1 = ((bf16[16,16,128]{2,1,0:T(8,128)(2,1)}), bf16[16,16,128]{2,1,0:T(8,128)(2,1)S(1)}, u32[]{:S(2)}, u32[]{:S(2)}) async-start(bf16[16,16,128]{2,1,0:T(8,128)(2,1)} %bitcast.12), calls=%async_computation.1 | async-start | bytes 131072 | tf_op jit(solution)/shard_map/all_to_all | solution.py:164
  152.6 92.9 %all-gather.5.cloned.1.call-start = ((), (), s32[]{:S(2)}) async-start(), calls=%async_computation.6 | async-start | bytes 4456448 | tf_op jit(solution)/shard_map/all_gather | solution.py:194
  159.3 86.2 %copy-start.6 = (bf16[1,2048,256]{2,1,0:T(8,128)(2,1)S(1)}, bf16[1,2048,256]{2,1,0:T(8,128)(2,1)}, u32[]{:S(2)}) copy-start(bf16[1,2048,256]{2,1,0:T(8,128)(2,1)} %param.25) | copy-start | bytes 3145732
  314.1 18.4 %copy-start.5 = (f32[16,2]{0,1:T(2,128)S(1)}, f32[16,2]{0,1:T(2,128)}, u32[]{:S(2)}) copy-start(f32[16,2]{0,1:T(2,128)} %param.24) | copy-start | bytes 388
  317.9 36.5 %all-to-all-start.4 = ((bf16[32,2,2048]{2,1,0:T(2,128)(2,1)}), bf16[32,2,2048]{2,1,0:T(2,128)(2,1)S(1)}, u32[]{:S(2)}, u32[]{:S(2)}) async-start(bf16[32,2,2048]{2,1,0:T(2,128)(2,1)} %all_to_all.39), calls=%async_computation.4 | async-start | bytes 524288 | tf_op jit(solution)/shard_map/all_to_all | solution.py:203
Sparse Core Ops, SparseCore 0:
  11.5 86.4 all-gather.2
  191.3 54.1 all-gather.4
where the time goes:
time: 364 us; the launch traced here: 363 us
  waiting for transfers between devices  185 us (51%)
  blocking collectives  85.5 us (23%)
  matrix products  27.4 us (8%)
  starting transfers between devices  25.5 us (7%)
  local copies, waits for them, and re-layouts  17.3 us (5%)
  between operations  13.7 us (4%)
  other arithmetic  9 us (2%)
    all_gather x1, waiting for transfers between devices, side_by_side(): result, at, done = (lax.all_gather(both, axis, axis=dim, tiled=True), 0, [])  86.4 us
    all_to_all x1, blocking collectives, sent_and_summed(): tiles = lax.all_to_all(split_up(value, dim, peers), axis, 0, 0, tiled=True)  55 us
    all_gather x1, waiting for transfers between devices, local(): piece = lax.all_gather(arrived, 'tp', axis=0, tiled=True)  54.4 us
    all_to_all x1, blocking collectives, local(): lax.all_to_all(send_rows, 'sp', split_axis=0, concat_axis=0, tiled=True)  30.5 us
    all_to_all x1, waiting for transfers between devices, local(): lax.all_to_all(expert_out, 'sp', split_axis=0, concat_axis=0, tiled=True)  21.9 us
    all_to_all x1, waiting for transfers between devices, copy_for_each(): return lax.all_to_all(copies, axis, split_axis=0, concat_axis=0, tiled=True)  15.7 us
    all_to_all x1, starting transfers between devices, local(): lax.all_to_all(expert_out, 'sp', split_axis=0, concat_axis=0, tiled=True)  14.3 us
    slice x3, local copies, waits for them, and re-layouts, side_by_side(): done.append(lax.slice_in_dim(result, at, at + a.shape[along], axis=along))  10.5 us
  transfers between devices with their start and end apart: 5, of which 5 were waited for; matrix products, arithmetic and copies ran while one was open for 0% of the time, Pallas kernels for 0%

commit v1 on v0

--- a/solution.py
+++ b/solution.py
@@ -191,7 +191,9 @@
     gate_weight = w_gate[0]
     up_weight = w_up[0]
     down_weight = w_down[0]
-    piece = lax.all_gather(arrived, "tp", axis=0, tiled=True)
+    opened = tuple((arrived for _ in range(jax.lax.psum(1, axis_name="tp"))))
+    item_now = jnp.concatenate(opened, axis=0)
+    piece = jax.lax.all_to_all(item_now, "tp", split_axis=0, concat_axis=0, tiled=True)
     gate = jnp.dot(piece, gate_weight, preferred_element_type=jnp.float32)
     upper = jnp.dot(piece, up_weight, preferred_element_type=jnp.float32)
     hidden = (jax.nn.silu(gate) * upper).astype(jnp.bfloat16)

time: 364 us -> 356 us (0.978)
  waiting for transfers between devices: 185 us -> 131 us
  blocking collectives: 85.5 us -> 138 us
  starting transfers between devices: 25.5 us -> 18.2 us
    all_gather x1 -> x0, waiting for transfers between devices: 54.4 us -> none  [local(): piece = lax.all_gather(arrived, 'tp', axis=0, tiled=True)]
    all_to_all x0 -> x1, blocking collectives: none -> 52.8 us  [local(): jax.lax.all_to_all(item_now, 'tp', split_axis=0, concat_axis=0, tiled=True)]
    all_to_all x1, starting transfers between devices: 14.3 us -> 7.21 us  [local(): lax.all_to_all(expert_out, 'sp', split_axis=0, concat_axis=0, tiled=True)]
  transfers between devices with their start and end apart: 5 -> 4, of which waited for: 5 -> 4; matrix products, arithmetic and copies ran while one was open for 0% -> 0% of each run, Pallas kernels for 0% -> 0%
where the time goes in v1:
time: 356 us; the launch traced here: 355 us
  blocking collectives  138 us (39%)
  waiting for transfers between devices  131 us (37%)
  matrix products  26.3 us (7%)
  local copies, waits for them, and re-layouts  18.9 us (5%)
  starting transfers between devices  18.2 us (5%)
  between operations  13.8 us (4%)
  other arithmetic  9 us (3%)
    all_gather x1, waiting for transfers between devices, side_by_side(): result, at, done = (lax.all_gather(both, axis, axis=dim, tiled=True), 0, [])  86.4 us
    all_to_all x1, blocking collectives, sent_and_summed(): tiles = lax.all_to_all(split_up(value, dim, peers), axis, 0, 0, tiled=True)  54.3 us
    all_to_all x1, blocking collectives, local(): jax.lax.all_to_all(item_now, 'tp', split_axis=0, concat_axis=0, tiled=True)  52.8 us
    all_to_all x1, blocking collectives, local(): lax.all_to_all(send_rows, 'sp', split_axis=0, concat_axis=0, tiled=True)  30.5 us
    all_to_all x1, waiting for transfers between devices, local(): lax.all_to_all(expert_out, 'sp', split_axis=0, concat_axis=0, tiled=True)  21.9 us
    all_to_all x1, waiting for transfers between devices, copy_for_each(): return lax.all_to_all(copies, axis, split_axis=0, concat_axis=0, tiled=True)  15.7 us
    slice x3, local copies, waits for them, and re-layouts, side_by_side(): done.append(lax.slice_in_dim(result, at, at + a.shape[along], axis=along))  10.5 us
    dot_general x1, matrix products, local(): jnp.dot(hidden, down_weight, preferred_element_type=jnp.float32)  9.05 us
  transfers between devices with their start and end apart: 4, of which 4 were waited for; matrix products, arithmetic and copies ran while one was open for 0% of the time, Pallas kernels for 0%

profile of v1, /device:TPU:1, one launch (start us, length us, event | category | flops | bytes accessed | tf_op | source)
XLA Modules:
  0.0 354.5 jit_solution(7381393774509043917)
XLA Ops:
  11.5 86.4 %all-gather.2.cloned.1.call-done = bf16[8192,256]{0,1:T(8,128)(2,1)} async-done(((bf16[256,256]{0,1:T(8,128)(2,1)}), bf16[8192,256]{0,1:T(8,128)(2,1)}) %all-gather.2.cloned.1.call-update) | async-done | bytes 4194320 | tf_op jit(solution)/shard_map/all_gather | solution.py:14
  97.9 3.9 %fusion.82 = (bf16[8192,128]{0,1:T(8,128)(2,1)S(1)}, bf16[8192,128]{0,1:T(8,128)(2,1)}) fusion(bf16[8192,256]{0,1:T(8,128)(2,1)} %all-gather.2.cloned.1.call-done), kind=kLoop, calls=%fused_computation.148 | loop fusion | bytes 8388608 | tf_op jit(solution)/shard_map/slice | solution.py:16
  101.8 4.1 %copy.35 = bf16[8192,128]{1,0:T(8,128)(2,1)} copy(bf16[8192,128]{0,1:T(8,128)(2,1)} %get-tuple-element.113) | data formatting | bytes 4194304 | tf_op jit(solution)/shard_map/slice | solution.py:16
  105.9 2.4 copy.37
  108.4 14.2 %while.15 = (s32[]{:T(128)}, f32[1,256]{1,0:T(1,128)S(1)}, f32[1,256]{1,0:T(1,128)S(1)}, f32[1,256,128]{2,1,0:T(8,128)S(1)}, bf16[4,2048,1,128]{3,1,2,0:T(8,128)...) while((s32[]{:T(128)}, f32[1,256]{1,0:T(1,128)S(1)}, ...), condition=%wide.region_5.6_spmd.clone, body=%wide.region_2.5_spmd.clone.sunk | while | flops 272729344 | bytes 7685225 | solution.py:105
  108.4 1.6 fusion.94
  110.4 1.6 fusion.97
  113.9 1.6 fusion.97
  117.5 1.6 fusion.97
  121.0 1.6 fusion.97
  123.9 6.5 %all-to-all-start = ((bf16[16,256,128]{1,2,0:T(8,128)(2,1)}), bf16[16,256,128]{1,2,0:T(8,128)(2,1)S(1)}, u32[]{:S(2)}, u32[]{:S(2)}) async-start(bf16[16,256,128]{1,2,0:T(8,128)(2,1)} %broadcast_in_dim.18), calls=%async_computation | async-start | bytes 2097152 | tf_op jit(solution)/shard_map/all_to_all | solution.py:29
  131.2 15.7 %all-to-all-done = bf16[16,256,128]{1,2,0:T(8,128)(2,1)S(1)} async-done(((bf16[16,256,128]{1,2,0:T(8,128)(2,1)}), bf16[16,256,128]{1,2,0:T(8,128)(2,1)S(1)}, u32[]{:S(2)}, u32[]{:S(2)}) %all-to-all-start) | async-done | bytes 1048608 | tf_op jit(solution)/shard_map/all_to_all | solution.py:29
  146.9 2.2 convolution_convert_fusion.2
  149.1 4.5 %all-to-all-start.1 = ((bf16[16,16,128]{2,1,0:T(8,128)(2,1)}), bf16[16,16,128]{2,1,0:T(8,128)(2,1)S(1)}, u32[]{:S(2)}, u32[]{:S(2)}) async-start(bf16[16,16,128]{2,1,0:T(8,128)(2,1)} %bitcast.12), calls=%async_computation.1 | async-start | bytes 131072 | tf_op jit(solution)/shard_map/all_to_all | solution.py:164
  153.6 6.5 %all-to-all-done.1 = bf16[16,16,128]{2,1,0:T(8,128)(2,1)S(1)} async-done(((bf16[16,16,128]{2,1,0:T(8,128)(2,1)}), bf16[16,16,128]{2,1,0:T(8,128)(2,1)S(1)}, u32[]{:S(2)}, u32[]{:S(2)}) %all-to-all-start.1) | async-done | bytes 65568 | tf_op jit(solution)/shard_map/all_to_all | solution.py:164
  160.7 30.5 %all_to_all.59 = bf16[32,2,2048]{2,1,0:T(2,128)(2,1)S(1)} all-to-all(bf16[32,2,2048]{2,1,0:T(2,128)(2,1)S(1)} %all_to_all.43), channel_id=1, replica_groups=mesh['sp'=32,'tp'=16] {'sp'}, dimensions={0} | all-to-all | bytes 524288 | tf_op jit(solution)/shard_map/all_to_all | solution.py:190
  191.8 52.8 %all_to_all.60 = bf16[16,64,2048]{2,1,0:T(8,128)(2,1)S(1)} all-to-all(bf16[16,64,2048]{2,1,0:T(8,128)(2,1)S(1)} %bitcast.93), channel_id=1, replica_groups=mesh['sp'=32,'tp'=16] {'tp'}, dimensions={0} | all-to-all | bytes 8388608 | tf_op jit(solution)/shard_map/all_to_all | solution.py:196
  244.6 2.0 copy-done.1
  246.5 2.3 fusion.15
  248.9 9.1 %convolution_convert_fusion = bf16[1024,2048]{1,0:T(8,128)(2,1)} fusion(bf16[1024,2048]{1,0:T(8,128)(2,1)} %bitcast.95, bf16[1,256,2048]{2,1,0:T(8,128)(2,1)S(1)} %copy-done, bf16[1,2048,256]{2,1,0:T(8,128)(2,1)} %param.26, f32[1024,256]{1,0:T(8,128)} %fusion.15), kind=kOutput, calls=%fused_computation.20 | convolution fusion | flops 2151153664 | bytes 11534336 | tf_op jit(solution)/shard_map/dot_general | solution.py:201
  257.9 54.3 %all_to_all.61 = bf16[16,64,2048]{2,1,0:T(8,128)(2,1)} all-to-all(bf16[16,64,2048]{2,1,0:T(8,128)(2,1)} %bitcast.96), channel_id=1, replica_groups=mesh['sp'=32,'tp'=16] {'tp'}, dimensions={0} | all-to-all | bytes 8388608 | tf_op jit(solution)/shard_map/all_to_all | solution.py:43
  312.3 3.0 reduce_sum.90
  316.1 7.2 %all-to-all-start.5 = ((bf16[32,2,2048]{2,1,0:T(2,128)(2,1)}), bf16[32,2,2048]{2,1,0:T(2,128)(2,1)S(1)}, u32[]{:S(2)}, u32[]{:S(2)}) async-start(bf16[32,2,2048]{2,1,0:T(2,128)(2,1)} %all_to_all.50), calls=%async_computation.5 | async-start | bytes 524288 | tf_op jit(solution)/shard_map/all_to_all | solution.py:205
  323.7 21.9 %all-to-all-done.5 = bf16[32,2,2048]{2,1,0:T(2,128)(2,1)S(1)} async-done(((bf16[32,2,2048]{2,1,0:T(2,128)(2,1)}), bf16[32,2,2048]{2,1,0:T(2,128)(2,1)S(1)}, u32[]{:S(2)}, u32[]{:S(2)}) %all-to-all-start.5) | async-done | bytes 262176 | tf_op jit(solution)/shard_map/all_to_all | solution.py:205
  (100 shorter events, 17.5 us)
Async XLA Ops:
  6.5 242.3 %copy-start = (bf16[1,256,2048]{2,1,0:T(8,128)(2,1)S(1)}, bf16[1,256,2048]{2,1,0:T(8,128)(2,1)}, u32[]{:S(2)}) copy-start(bf16[1,256,2048]{2,1,0:T(8,128)(2,1)} %param.27) | copy-start | bytes 3145732
  6.5 91.4 %all-gather.2.cloned.1.call-start = ((), (), s32[]{:S(2)}) async-start(), calls=%async_computation.6 | async-start | bytes 4325376 | tf_op jit(solution)/shard_map/all_gather | solution.py:14
  108.4 22.1 %copy-start.3 = (s32[16,2]{0,1:T(2,128)S(1)}, s32[16,2]{0,1:T(2,128)}, u32[]{:S(2)}) copy-start(s32[16,2]{0,1:T(2,128)} %param.23) | copy-start | bytes 388
  122.6 37.5 %copy-start.2 = (bf16[16,2048]{1,0:T(8,128)(2,1)S(1)}, bf16[16,2048]{1,0:T(8,128)(2,1)}, u32[]{:S(2)}) copy-start(bf16[16,2048]{1,0:T(8,128)(2,1)} %param.22) | copy-start | bytes 196612
  122.6 37.6 %copy-start.4 = (f32[2048]{0:T(1024)S(1)}, f32[2048]{0:T(1024)}, u32[]{:S(2)}) copy-start(f32[2048]{0:T(1024)} %param.21) | copy-start | bytes 24580
  123.9 23.0 %all-to-all-start = ((bf16[16,256,128]{1,2,0:T(8,128)(2,1)}), bf16[16,256,128]{1,2,0:T(8,128)(2,1)S(1)}, u32[]{:S(2)}, u32[]{:S(2)}) async-start(bf16[16,256,128]{1,2,0:T(8,128)(2,1)} %broadcast_in_dim.18), calls=%async_computation | async-start | bytes 2097152 | tf_op jit(solution)/shard_map/all_to_all | solution.py:29
  149.1 11.0 %all-to-all-start.1 = ((bf16[16,16,128]{2,1,0:T(8,128)(2,1)}), bf16[16,16,128]{2,1,0:T(8,128)(2,1)S(1)}, u32[]{:S(2)}, u32[]{:S(2)}) async-start(bf16[16,16,128]{2,1,0:T(8,128)(2,1)} %bitcast.12), calls=%async_computation.1 | async-start | bytes 131072 | tf_op jit(solution)/shard_map/all_to_all | solution.py:164
  191.8 54.8 %copy-start.6 = (bf16[1,2048,256]{2,1,0:T(8,128)(2,1)S(1)}, bf16[1,2048,256]{2,1,0:T(8,128)(2,1)}, u32[]{:S(2)}) copy-start(bf16[1,2048,256]{2,1,0:T(8,128)(2,1)} %param.25) | copy-start | bytes 3145732
  244.6 2.0 copy-start.1
  312.3 11.4 %copy-start.5 = (f32[16,2]{0,1:T(2,128)S(1)}, f32[16,2]{0,1:T(2,128)}, u32[]{:S(2)}) copy-start(f32[16,2]{0,1:T(2,128)} %param.24) | copy-start | bytes 388
  316.1 29.5 %all-to-all-start.5 = ((bf16[32,2,2048]{2,1,0:T(2,128)(2,1)}), bf16[32,2,2048]{2,1,0:T(2,128)(2,1)S(1)}, u32[]{:S(2)}, u32[]{:S(2)}) async-start(bf16[32,2,2048]{2,1,0:T(2,128)(2,1)} %all_to_all.50), calls=%async_computation.5 | async-start | bytes 524288 | tf_op jit(solution)/shard_map/all_to_all | solution.py:205
Sparse Core Ops, SparseCore 0:
  11.5 86.4 all-gather.1
